TPU v7x, 32 devices: a whole 2x2x4 slice. The times are simulated.
32 devices in a mesh: grp: 2 (over y), dp: 2 (over x), kv: 4 (over z), tp: 2 (over core).
Axes of the slice: x: 2, y: 2, z: 4, core: 2. Of those that a mesh axis runs over, the one named last changes fastest.
Arguments:
- queries: bfloat16 [4, 1024, 2048], P(('grp', 'dp'), 'kv', 'tp'), parts along dimension 0, may hold values from -10 to 10
- keys: bfloat16 [4, 1024, 512], P(('grp', 'dp'), 'kv', 'tp'), parts along dimension 0, may hold values from -10 to 10
- values: bfloat16 [4, 1024, 512], P(('grp', 'dp'), 'kv', 'tp'), parts along dimension 0, may hold values from -6 to 6
- gate_logits: float32 [4, 2, 1024, 32], P(('grp', 'dp'), None, 'kv', 'tp'), parts along dimension 0, may hold values from -6 to 6
- chosen: int32 [4, 8, 8, 16], P(('grp', 'dp'), 'kv', 'tp'), parts along dimension 0, may hold values from -1 to 15, as said below
- pool_k: float32 [32, 64], replicated, may hold values from 0 to 0.35
- pool_v: float32 [32, 64], replicated, may hold values from 0 to 0.35
- out_gain: float32 [2048], P('tp'), may hold values from 0.1 to 1.9
Outputs:
- attended: bfloat16 [4, 1024, 2048], P(('grp', 'dp'), 'kv', 'tp'), parts along dimension 0
There are 2 independent parts, one for each index of `grp`. A program takes and returns all parts, laid end to end along the dimension named above; an argument that names none is the same for every part. Nothing has to cross between parts.
Inputs may be any that keep to these rules, and one draw needn't show every extreme that they name: Entries are key block numbers (block e holds positions e * 64 to e * 64 + 63) or -1 for none. The list of query block b (positions b * 128 onward) holds the blocks that contain its own positions, other distinct blocks that begin before it, and -1 in its remaining entries. For the query blocks of one span of 256 positions and one key head, the blocks chosen from any other span number at most 2; in every draw some span reaches 2.
All inputs are finite; a program needn't handle non-finite values.
Results may differ from a plain program's by a relative error of at most 0.0079.
Values may be sent and summed in bfloat16 or wider, within the bound.
A program may use at most 64 MiB of HBM per device.

v0:
```python
import jax
import jax.numpy as jnp
from jax import lax
from jax.sharding import PartitionSpec as P

DH = 64
CMP_STRIDE = 16
CMP_BLOCK = 32
SLC = 64
QB = 128
NSEL = 16
MOST = 2
THETA = 500000.0
EPS = 1e-06
NEG = -1e30


def shifted(block, axis, distance):
    devices = range(lax.axis_size(axis))
    route = [(i - distance, i) for i in devices if i - distance in devices]
    return lax.ppermute(block, axis, route)


def rotate(matrix, start, heads):
    length = matrix.shape[0]
    half = DH // 2
    place = (start + jnp.arange(length)).astype(jnp.float32)
    freq = jnp.power(jnp.float32(THETA), -(2.0 * jnp.arange(half).astype(jnp.float32)) / DH)
    angle = place[:, None] * freq[None, :]
    cosine = jnp.cos(angle)[:, None, :]
    sine = jnp.sin(angle)[:, None, :]
    parts = matrix.reshape(length, heads, DH).astype(jnp.float32)
    first = parts[..., :half]
    second = parts[..., half:]
    turned = jnp.concatenate([first * cosine - second * sine, second * cosine + first * sine], -1)
    return turned.reshape(length, heads * DH).astype(jnp.bfloat16)


def compress(extended, pool, groups):
    count = extended.shape[0] // CMP_STRIDE - 1
    parts = extended.reshape(count + 1, CMP_STRIDE, groups, DH).astype(jnp.float32)
    lower = jnp.einsum(
        "nigd,id->ngd", parts[:-1], pool[:CMP_STRIDE], precision=lax.Precision.HIGHEST
    )
    upper = jnp.einsum(
        "nigd,id->ngd", parts[1:], pool[CMP_STRIDE:], precision=lax.Precision.HIGHEST
    )
    return (lower + upper).astype(jnp.bfloat16)


def wanted_blocks(lists, owners, per_owner):
    groups = lists.shape[1]
    total = owners * per_owner
    hits = lists[..., None] == jnp.arange(total, dtype=jnp.int32)
    member = jnp.any(hits, axis=(0, 2)).astype(jnp.int32).reshape(groups, owners, per_owner)
    rank = jnp.cumsum(member, -1) - member
    slot_hit = (member[..., None] == 1) & (rank[..., None] == jnp.arange(MOST))
    local_ids = jnp.arange(per_owner, dtype=jnp.int32)[:, None]
    asked = jnp.sum(jnp.where(slot_hit, local_ids, 0), axis=2)
    return (asked.transpose(1, 0, 2), rank.reshape(groups, total))


def per_device(queries, keys, values, gate_logits, chosen, pool_k, pool_v, out_gain):
    queries = queries[0]
    keys = keys[0]
    values = values[0]
    logits = gate_logits[0]
    lists = chosen[0]
    length = queries.shape[0]
    groups = keys.shape[1] // DH
    heads = queries.shape[1] // DH
    per_group = heads // groups
    qblocks = length // QB
    owners = lax.axis_size("kv")
    myself = lax.axis_index("kv")
    start = myself * length
    scale = DH ** (-0.5)
    query_turned = rotate(queries, start, heads)
    key_turned = rotate(keys, start, groups)
    next_keys, next_values = shifted((keys[:CMP_STRIDE], values[:CMP_STRIDE]), "kv", -1)
    key_summary = compress(jnp.concatenate([keys, next_keys], 0), pool_k, groups)
    value_summary = compress(jnp.concatenate([values, next_values], 0), pool_v, groups)
    place = start + jnp.arange(length)
    query_group = queries.reshape(length, groups, per_group, DH).transpose(1, 2, 0, 3)
    part_keys = lax.all_gather(key_summary, "kv", axis=0, tiled=True)
    part_values = lax.all_gather(value_summary, "kv", axis=0, tiled=True)
    count = part_keys.shape[0]
    ends = jnp.arange(count) * CMP_STRIDE + CMP_BLOCK - 1
    allow = ends[None, :] <= place[:, None]

    def per_group_fold(item):
        query_part, key_part, value_part, top, total, summed = item
        score = (
            jnp.einsum("htd,nd->htn", query_part, key_part, preferred_element_type=jnp.float32)
            * scale
        )
        score = jnp.where(allow, score, NEG)
        fresh = jnp.maximum(top, jnp.max(score, -1))
        weight = jnp.where(allow, jnp.exp(score - fresh[..., None]), 0.0)
        shrink = jnp.exp(top - fresh)
        total = total * shrink + jnp.sum(weight, -1)
        summed = summed * shrink[..., None] + jnp.einsum(
            "htn,nd->htd",
            weight.astype(jnp.bfloat16),
            value_part,
            preferred_element_type=jnp.float32,
        )
        return (fresh, total, summed)

    top = jnp.full((groups, per_group, length), NEG, jnp.float32)
    total = jnp.zeros((groups, per_group, length), jnp.float32)
    summed = jnp.zeros((groups, per_group, length, DH), jnp.float32)
    top, total, summed = lax.map(
        per_group_fold,
        (
            query_group,
            part_keys.transpose(1, 0, 2),
            part_values.transpose(1, 0, 2),
            top,
            total,
            summed,
        ),
    )
    summary_out = summed / jnp.maximum(total, 1.0)[..., None]
    group_pick = jnp.arange(groups)[None, :, None]
    safe = jnp.maximum(lists, 0)
    per_owner = length // SLC
    asked_ids, rank = wanted_blocks(lists, owners, per_owner)
    requests = lax.all_to_all(asked_ids, "kv", split_axis=0, concat_axis=0, tiled=True)
    local_keys = key_turned.reshape(per_owner, SLC, groups, DH)
    local_values = values.reshape(per_owner, SLC, groups, DH)
    served = (local_keys[requests, :, group_pick, :], local_values[requests, :, group_pick, :])
    got_keys, got_values = (
        lax.all_to_all(served[0], "kv", split_axis=0, concat_axis=0, tiled=True),
        lax.all_to_all(served[1], "kv", split_axis=0, concat_axis=0, tiled=True),
    )

    def table(received, local):
        remote = received.transpose(1, 0, 2, 3, 4).reshape(groups, owners * MOST, SLC, DH)
        return jnp.concatenate([remote, local.transpose(2, 0, 1, 3)], 1)

    owner = safe // per_owner
    inner = safe % per_owner
    slot = jnp.where(owner == myself, owners * MOST + inner, owner * MOST + rank[group_pick, safe])
    key_sel = table(got_keys, local_keys)[group_pick, slot]
    value_sel = table(got_values, local_values)[group_pick, slot]
    query_blocks = query_turned.reshape(qblocks, QB, groups, per_group, DH)

    def attend(item):
        index, query_part, keys_part, values_part, picks = item
        place_q = start + index * QB + jnp.arange(QB)
        score = jnp.einsum(
            "tghd,gnkd->ghtnk", query_part, keys_part, preferred_element_type=jnp.float32
        )
        score = score.reshape(groups, per_group, QB, NSEL * SLC) * scale
        safe_picks = jnp.maximum(picks, 0)
        key_place = (safe_picks[..., None] * SLC + jnp.arange(SLC)).reshape(groups, NSEL * SLC)
        live = jnp.broadcast_to(picks[..., None] >= 0, (groups, NSEL, SLC)).reshape(
            groups, NSEL * SLC
        )
        allow = (live[:, None, :] & (key_place[:, None, :] <= place_q[None, :, None]))[:, None]
        score = jnp.where(allow, score, NEG)
        top_sel = jnp.max(score, -1, keepdims=True)
        weight = jnp.where(allow, jnp.exp(score - top_sel), 0.0)
        total_sel = jnp.sum(weight, -1)
        flat_values = values_part.reshape(groups, NSEL * SLC, DH)
        out = jnp.einsum(
            "ghtk,gkd->ghtd",
            weight.astype(jnp.bfloat16),
            flat_values,
            preferred_element_type=jnp.float32,
        )
        return out / total_sel[..., None]

    chosen_out = lax.map(attend, (jnp.arange(qblocks), query_blocks, key_sel, value_sel, lists))
    gates = jax.nn.sigmoid(logits)
    summary_rows = summary_out.transpose(2, 0, 1, 3).reshape(length, heads, DH)
    chosen_rows = chosen_out.transpose(0, 3, 1, 2, 4).reshape(length, heads, DH)
    mixed = gates[0][..., None] * summary_rows + gates[1][..., None] * chosen_rows
    normed = (
        mixed
        * lax.rsqrt(jnp.mean(mixed * mixed, -1, keepdims=True) + EPS)
        * out_gain.reshape(heads, DH)
    )
    return normed.reshape(1, length, heads * DH).astype(jnp.bfloat16)


def solution(mesh):
    in_specs = (
        P(("grp", "dp"), "kv", "tp"),
        P(("grp", "dp"), "kv", "tp"),
        P(("grp", "dp"), "kv", "tp"),
        P(("grp", "dp"), None, "kv", "tp"),
        P(("grp", "dp"), "kv", "tp", None),
        P(),
        P(),
        P("tp"),
    )
    out_specs = P(("grp", "dp"), "kv", "tp")
    return jax.shard_map(
        per_device, mesh=mesh, in_specs=in_specs, out_specs=out_specs, check_vma=False
    )
```

profile of v0, /device:TPU:0, one launch (start us, length us, event | category | flops | bytes accessed | tf_op | source)
XLA Modules:
  0.0 114.5 jit_solution(15482757723917872336)
XLA Ops:
  2.6 6.3 %all-to-all-start = ((s32[4,4,2]{1,2,0:T(2,128)}), s32[4,4,2]{1,2,0:T(2,128)S(1)}, u32[]{:S(2)}, u32[]{:S(2)}) async-start(s32[4,4,2]{1,2,0:T(2,128)} %copy.74), calls=%async_computation | async-start | bytes 8192 | tf_op jit(solution)/shard_map/all_to_all | solution.py:129
  9.6 1.3 %collective-permute-start.1 = (bf16[16,256]{1,0:T(8,128)(2,1)S(1)}, bf16[16,256]{1,0:T(8,128)(2,1)S(1)}, u32[]{:S(2)}, u32[]{:S(2)}) collective-permute-start(bf16[16,256]{1,0:T(8,128)(2,1)S(1)} %slice_bitcast_fusion.1), channel_id=1, source_target_pairs={{2,0},{4,2},{6,4},{3,1},{5,3},{7,5},{10,8},{12,10},{14,12},{11,9},... | collective-permute-start | bytes 24584 | tf_op jit(solution)/shard_map/ppermute | solution.py:21
  11.6 1.3 %collective-permute-start = (bf16[16,256]{1,0:T(8,128)(2,1)S(1)}, bf16[16,256]{1,0:T(8,128)(2,1)S(1)}, u32[]{:S(2)}, u32[]{:S(2)}) collective-permute-start(bf16[16,256]{1,0:T(8,128)(2,1)S(1)} %slice_bitcast_fusion.4), channel_id=1, source_target_pairs={{2,0},{4,2},{6,4},{3,1},{5,3},{7,5},{10,8},{12,10},{14,12},{11,9},... | collective-permute-start | bytes 24584 | tf_op jit(solution)/shard_map/ppermute | solution.py:21
  13.7 1.0 copy.73
  14.8 1.1 reshape_squeeze.9
  15.8 1.1 slice.65
  16.9 1.1 slice.72
  18.1 1.5 %gather_fusion.1 = s32[128]{0:T(128)S(1)} fusion(s32[4,16]{1,0:T(4,128)S(1)} %convert_subtract_fusion, s32[128]{0:T(128)S(1)} %reshape.454), kind=kCustom, calls=%fused_computation.1 | custom fusion | bytes 2048 | tf_op jit(solution)/shard_map/gather | solution.py:144
  26.7 1.1 reshape.513
  27.8 7.4 %all-to-all-start.2 = ((bf16[4,2,16384]{2,1,0:T(2,128)(2,1)}), bf16[4,2,16384]{2,1,0:T(2,128)(2,1)S(1)}, u32[]{:S(2)}, u32[]{:S(2)}) async-start(bf16[4,2,16384]{2,1,0:T(2,128)(2,1)} %reshape.513), calls=%async_computation.2 | async-start | bytes 524288 | tf_op jit(solution)/shard_map/all_to_all | solution.py:135
  35.9 1.1 reshape.511
  37.6 13.7 %all_gather.7 = bf16[64,4,64]{2,1,0:T(4,128)(2,1)S(1)} all-gather(bf16[16,4,64]{2,1,0:T(4,128)(2,1)S(1)} %fusion.39), channel_id=1, replica_groups=mesh['grp'=2,'dp'=2,'kv'=4,'tp'=2] {'kv'}, dimensions={0}, use_global_device_ids=true | all-gather | bytes 40960 | tf_op jit(solution)/shard_map/all_gather | solution.py:86
  51.6 13.3 %all_gather.6 = bf16[64,4,64]{2,0,1:T(8,128)(2,1)S(1)} all-gather(bf16[16,4,64]{2,0,1:T(8,128)(2,1)S(1)} %fusion.40), channel_id=1, replica_groups=mesh['grp'=2,'dp'=2,'kv'=4,'tp'=2] {'kv'}, dimensions={0}, use_global_device_ids=true | all-gather | bytes 40960 | tf_op jit(solution)/shard_map/all_gather | solution.py:85
  64.9 4.6 %all-to-all-start.1 = ((bf16[4,2,16384]{2,1,0:T(2,128)(2,1)}), bf16[4,2,16384]{2,1,0:T(2,128)(2,1)S(1)}, u32[]{:S(2)}, u32[]{:S(2)}) async-start(bf16[4,2,16384]{2,1,0:T(2,128)(2,1)} %reshape.511), calls=%async_computation.1 | async-start | bytes 524288 | tf_op jit(solution)/shard_map/all_to_all | solution.py:134
  69.5 5.2 %while.24 = (s32[]{:T(128)}, f32[4,4,256]{2,1,0:T(4,128)S(1)}, f32[4,4,256,64]{2,3,1,0:T(8,128)}, bf16[4,4,256,64]{2,3,1,0:T(8,128)(2,1)S(1)}, bf16[4,64,64]{2,1...) while((s32[]{:T(128)}, f32[4,4,256]{2,1,0:T(4,128)S(1)}, ...), condition=%wide.region_3.4_spmd.clone, body=%wide.region_0.3_spmd.clone.sunk | while | flops 17454080 | bytes 1326441 | solution.py:113
  75.1 1.2 %all-to-all-done.1 = bf16[4,2,16384]{2,1,0:T(2,128)(2,1)S(1)} async-done(((bf16[4,2,16384]{2,1,0:T(2,128)(2,1)}), bf16[4,2,16384]{2,1,0:T(2,128)(2,1)S(1)}, u32[]{:S(2)}, u32[]{:S(2)}) %all-to-all-start.1) | async-done | bytes 262176 | tf_op jit(solution)/shard_map/all_to_all | solution.py:134
  77.0 2.3 %gather_fusion.2 = bf16[128,64,64]{2,1,0:T(8,128)(2,1)} fusion(bf16[4,12,64,64]{3,2,1,0:T(8,128)(2,1)S(1)} %pad_maximum_fusion, s32[128]{0:T(128)S(1)} %reshape.460), kind=kCustom, calls=%fused_computation.2 | custom fusion | bytes 2098176 | tf_op jit(solution)/shard_map/gather | solution.py:145
  79.3 1.1 gather_fusion.4
  80.5 28.3 %while.23 = (s32[]{:T(128)}, f32[2,4,4,128,64]{3,4,2,1,0:T(8,128)}, s32[2,4,16]{2,1,0:T(4,128)S(1)}, s32[2]{0:T(128)S(1)}, s32[]{:T(128)}, /*index=5*/bf16[2,4,1...) while((s32[]{:T(128)}, f32[2,4,4,128,64]{3,4,2,1,0:T(8,128)}, ...), condition=%wide.region_10.11_spmd, body=%wide.region_7.10_spmd.sunk | while | flops 562172224 | bytes 65482908 | solution.py:175
  83.3 1.4 %compare_and_fusion.5 = pred[4,128,1024]{1,2,0:T(8,128)(4,1)S(1)} fusion(s32[128]{0:T(128)S(1)} %iota_add_fusion.5, s32[4,1024]{1,0:T(4,128)S(1)} %broadcast_add_fusion.2, pred[4,1024]{1,0:T(4,128)(4,1)S(1)} %and.110), kind=kLoop, calls=%fused_computation.15.clone.1 | loop fusion | flops 1048576 | bytes 545280 | tf_op jit(solution)/shard_map/while/body/eval_jaxpr/and | solution.py:161
  84.8 2.5 %select_reduce_fusion.5 = (f32[4,4,128]{2,1,0:T(4,128)S(1)}, f32[4,4,128,16,64]{2,4,1,3,0:T(8,128)S(1)}) fusion(pred[4,128,16,64]{1,3,2,0:T(8,128)(4,1)S(1)} %compare_and_fusion.4, bf16[2,128,4,4,64]{1,4,3,2,0:T(8,128)(2,1)} %get-tuple-element.346, s32[]{:T(128)S(6)} %copy.143, bf16[2,4,16,64,64]{4,3,2,1,0:T(8,128)(2,1)} %get-tuple-element.345), kind=kOutput, calls=%fused_computation.13.clone.1 | convolution fusion | flops 274724864 | bytes 10232832 | tf_op jit(solution)/shard_map/while/body/eval_jaxpr/tghd,gnkd->ghtnk/dot_general | solution.py:152
  87.3 2.1 %select_reduce_fusion.6 = f32[4,4,128]{2,1,0:T(4,128)S(1)} fusion(f32[4,4,128,16,64]{2,4,1,3,0:T(8,128)S(1)} %get-tuple-element.306, f32[4,4,128]{2,1,0:T(4,128)S(1)} %get-tuple-element.307, pred[4,128,16,64]{1,3,2,0:T(8,128)(4,1)S(1)} %compare_and_fusion.4), kind=kLoop, calls=%fused_computation.11.clone.1 | loop fusion | flops 8386560 | bytes 8929280 | tf_op jit(solution)/shard_map/while/body/eval_jaxpr/reduce_sum | solution.py:165
  90.3 2.4 %fusion.68 = bf16[4,4,128,1024]{2,3,1,0:T(8,128)(2,1)S(1)} fusion(f32[4,4,128,16,64]{2,4,3,1,0:T(8,128)S(1)} %copy.137, f32[4,4,128]{2,1,0:T(4,128)S(1)} %get-tuple-element.307, pred[4,128,1024]{1,2,0:T(8,128)(4,1)S(1)} %compare_and_fusion.5), kind=kLoop, calls=%fused_computation.10.clone.1 | loop fusion | flops 8388608 | bytes 13115392 | tf_op jit(solution)/shard_map/while/body/eval_jaxpr/convert_element_type | solution.py:169
  93.6 1.0 copy-done.1
  97.4 1.4 %compare_and_fusion.5 = pred[4,128,1024]{1,2,0:T(8,128)(4,1)S(1)} fusion(s32[128]{0:T(128)S(1)} %iota_add_fusion.5, s32[4,1024]{1,0:T(4,128)S(1)} %broadcast_add_fusion.2, pred[4,1024]{1,0:T(4,128)(4,1)S(1)} %and.110), kind=kLoop, calls=%fused_computation.15.clone.1 | loop fusion | flops 1048576 | bytes 545280 | tf_op jit(solution)/shard_map/while/body/eval_jaxpr/and | solution.py:161
  98.9 2.5 %select_reduce_fusion.5 = (f32[4,4,128]{2,1,0:T(4,128)S(1)}, f32[4,4,128,16,64]{2,4,1,3,0:T(8,128)S(1)}) fusion(pred[4,128,16,64]{1,3,2,0:T(8,128)(4,1)S(1)} %compare_and_fusion.4, bf16[2,128,4,4,64]{1,4,3,2,0:T(8,128)(2,1)} %get-tuple-element.346, s32[]{:T(128)S(6)} %copy.143, bf16[2,4,16,64,64]{4,3,2,1,0:T(8,128)(2,1)} %get-tuple-element.345), kind=kOutput, calls=%fused_computation.13.clone.1 | convolution fusion | flops 274724864 | bytes 10232832 | tf_op jit(solution)/shard_map/while/body/eval_jaxpr/tghd,gnkd->ghtnk/dot_general | solution.py:152
  101.4 2.1 %select_reduce_fusion.6 = f32[4,4,128]{2,1,0:T(4,128)S(1)} fusion(f32[4,4,128,16,64]{2,4,1,3,0:T(8,128)S(1)} %get-tuple-element.306, f32[4,4,128]{2,1,0:T(4,128)S(1)} %get-tuple-element.307, pred[4,128,16,64]{1,3,2,0:T(8,128)(4,1)S(1)} %compare_and_fusion.4), kind=kLoop, calls=%fused_computation.11.clone.1 | loop fusion | flops 8386560 | bytes 8929280 | tf_op jit(solution)/shard_map/while/body/eval_jaxpr/reduce_sum | solution.py:165
  104.4 2.4 %fusion.68 = bf16[4,4,128,1024]{2,3,1,0:T(8,128)(2,1)S(1)} fusion(f32[4,4,128,16,64]{2,4,3,1,0:T(8,128)S(1)} %copy.137, f32[4,4,128]{2,1,0:T(4,128)S(1)} %get-tuple-element.307, pred[4,128,1024]{1,2,0:T(8,128)(4,1)S(1)} %compare_and_fusion.5), kind=kLoop, calls=%fused_computation.10.clone.1 | loop fusion | flops 8388608 | bytes 13115392 | tf_op jit(solution)/shard_map/while/body/eval_jaxpr/convert_element_type | solution.py:169
  107.7 1.0 copy-done.1
  108.7 1.6 %fusion.33 = (f32[256,4,4]{0,2,1:T(4,128)S(1)}, f32[4,4,256,64]{2,3,1,0:T(8,128)S(1)}) fusion(f32[256,4,4]{0,2,1:T(4,128)S(1)} %mul.290, f32[256,4,4]{0,2,1:T(4,128)S(1)} %mul.287, f32[4,4,256,64]{2,3,1,0:T(8,128)S(1)} %copy-done.4, f32[4,4,256]{2,1,0:T(4,128)S(1)} %broadcast_maximum_fusion.1, f32[2,4,4,128,64]{3,4,2,1,0:T(8,128)} %get-tuple-element.87), kind=kLoop, calls=%fused_computation.57 | loop fusion | flops 1568768 | bytes 3211264 | tf_op jit(solution)/shard_map/reduce_sum | solution.py:182
  110.3 2.0 %copy.86 = f32[2,128,4,4,64]{1,0,4,3,2:T(2,128)S(1)} copy(f32[2,128,4,4,64]{1,4,3,2,0:T(8,128)} %bitcast.233) | data formatting | bytes 2097152 | tf_op jit(solution)/shard_map/transpose | solution.py:178
  113.5 1.0 copy.88
  (152 shorter events, 28.4 us)
Async XLA Ops:
  0.0 23.6 %copy-start.5 = (bf16[1,256,1024]{2,1,0:T(8,128)(2,1)S(1)}, bf16[1,256,1024]{2,1,0:T(8,128)(2,1)}, u32[]{:S(2)}) copy-start(bf16[1,256,1024]{2,1,0:T(8,128)(2,1)} %param.12) | copy-start | bytes 1572868
  2.6 23.2 %all-to-all-start = ((s32[4,4,2]{1,2,0:T(2,128)}), s32[4,4,2]{1,2,0:T(2,128)S(1)}, u32[]{:S(2)}, u32[]{:S(2)}) async-start(s32[4,4,2]{1,2,0:T(2,128)} %copy.74), calls=%async_computation | async-start | bytes 8192 | tf_op jit(solution)/shard_map/all_to_all | solution.py:129
  9.6 27.4 %collective-permute-start.1 = (bf16[16,256]{1,0:T(8,128)(2,1)S(1)}, bf16[16,256]{1,0:T(8,128)(2,1)S(1)}, u32[]{:S(2)}, u32[]{:S(2)}) collective-permute-start(bf16[16,256]{1,0:T(8,128)(2,1)S(1)} %slice_bitcast_fusion.1), channel_id=1, source_target_pairs={{2,0},{4,2},{6,4},{3,1},{5,3},{7,5},{10,8},{12,10},{14,12},{11,9},... | collective-permute-start | bytes 24584 | tf_op jit(solution)/shard_map/ppermute | solution.py:21
  11.6 25.8 %collective-permute-start = (bf16[16,256]{1,0:T(8,128)(2,1)S(1)}, bf16[16,256]{1,0:T(8,128)(2,1)S(1)}, u32[]{:S(2)}, u32[]{:S(2)}) collective-permute-start(bf16[16,256]{1,0:T(8,128)(2,1)S(1)} %slice_bitcast_fusion.4), channel_id=1, source_target_pairs={{2,0},{4,2},{6,4},{3,1},{5,3},{7,5},{10,8},{12,10},{14,12},{11,9},... | collective-permute-start | bytes 24584 | tf_op jit(solution)/shard_map/ppermute | solution.py:21
  19.6 17.4 %copy-start.2 = (bf16[1,256,256]{2,1,0:T(8,128)(2,1)S(1)}, bf16[1,256,256]{2,1,0:T(8,128)(2,1)}, u32[]{:S(2)}) copy-start(bf16[1,256,256]{2,1,0:T(8,128)(2,1)} %param.14) | copy-start | bytes 393220
  22.8 14.6 %copy-start.3 = (bf16[1,256,256]{2,1,0:T(8,128)(2,1)S(1)}, bf16[1,256,256]{2,1,0:T(8,128)(2,1)}, u32[]{:S(2)}) copy-start(bf16[1,256,256]{2,1,0:T(8,128)(2,1)} %param.13) | copy-start | bytes 393220
  27.8 37.1 %all-to-all-start.2 = ((bf16[4,2,16384]{2,1,0:T(2,128)(2,1)}), bf16[4,2,16384]{2,1,0:T(2,128)(2,1)S(1)}, u32[]{:S(2)}, u32[]{:S(2)}) async-start(bf16[4,2,16384]{2,1,0:T(2,128)(2,1)} %reshape.513), calls=%async_computation.2 | async-start | bytes 524288 | tf_op jit(solution)/shard_map/all_to_all | solution.py:135
  64.9 11.4 %all-to-all-start.1 = ((bf16[4,2,16384]{2,1,0:T(2,128)(2,1)}), bf16[4,2,16384]{2,1,0:T(2,128)(2,1)S(1)}, u32[]{:S(2)}, u32[]{:S(2)}) async-start(bf16[4,2,16384]{2,1,0:T(2,128)(2,1)} %reshape.511), calls=%async_computation.1 | async-start | bytes 524288 | tf_op jit(solution)/shard_map/all_to_all | solution.py:134
  74.7 5.7 %copy-start.6 = (s32[1,2,4,16]{3,2,1,0:T(4,128)S(1)}, s32[1,2,4,16]{3,2,1,0:T(4,128)}, u32[]{:S(2)}) copy-start(s32[1,2,4,16]{3,2,1,0:T(4,128)} %param.16) | copy-start | bytes 1540
  80.4 28.3 %copy-start.4 = (f32[4,4,256,64]{2,3,1,0:T(8,128)S(1)}, f32[4,4,256,64]{2,3,1,0:T(8,128)}, u32[]{:S(2)}) copy-start(f32[4,4,256,64]{2,3,1,0:T(8,128)} %get-tuple-element.85) | copy-start | bytes 3145732
  80.4 32.8 %copy-start.7 = (f32[1024]{0:T(1024)S(1)}, f32[1024]{0:T(1024)}, u32[]{:S(2)}) copy-start(f32[1024]{0:T(1024)} %param.19) | copy-start | bytes 12292
  90.3 2.4 %copy-start = (f32[2,4,4,128,64]{3,4,2,1,0:T(8,128)S(1)}, f32[2,4,4,128,64]{3,4,2,1,0:T(8,128)}, u32[]{:S(2)}) copy-start(f32[2,4,4,128,64]{3,4,2,1,0:T(8,128)} %get-tuple-element.331) | copy-start | bytes 3145732 | tf_op jit(solution)/shard_map/while
  93.6 1.0 copy-start.1
  104.4 2.4 %copy-start = (f32[2,4,4,128,64]{3,4,2,1,0:T(8,128)S(1)}, f32[2,4,4,128,64]{3,4,2,1,0:T(8,128)}, u32[]{:S(2)}) copy-start(f32[2,4,4,128,64]{3,4,2,1,0:T(8,128)} %get-tuple-element.331) | copy-start | bytes 3145732 | tf_op jit(solution)/shard_map/while
  107.7 1.0 copy-start.1
where the time goes:
time: 115 us; the launch traced here: 114 us
  local copies, waits for them, and re-layouts  29.9 us (26%)
  blocking collectives  27 us (23%)
  other arithmetic  22.1 us (19%)
  starting transfers between devices  21 us (18%)
  matrix products  11.2 us (10%)
  loops' own time  1.71 us (1%)
  waiting for transfers between devices  1.22 us (1%)
    all_gather x1, blocking collectives, per_device(): part_values = lax.all_gather(value_summary, 'kv', axis=0, tiled=True)  13.7 us
    all_gather x1, blocking collectives, per_device(): part_keys = lax.all_gather(key_summary, 'kv', axis=0, tiled=True)  13.3 us
    all_to_all x1, starting transfers between devices, per_device(): lax.all_to_all(served[1], 'kv', split_axis=0, concat_axis=0, tiled=True)  7.44 us
    all_to_all x1, starting transfers between devices, per_device(): lax.all_to_all(asked_ids, 'kv', split_axis=0, concat_axis=0, tiled=True)  6.35 us
    unnamed x21, local copies, waits for them, and re-layouts  5.66 us
    dot_general x2, matrix products, attend(): jnp.einsum('tghd,gnkd->ghtnk', query_part, keys_part, preferred_element_t...  5.03 us
    convert_element_type x2, other arithmetic, attend(): weight.astype(jnp.bfloat16)  4.81 us
    and x4, other arithmetic, attend(): live[:, None, :] & (key_place[:, None, :] <= place_q[None, :, None])  4.65 us
  transfers between devices with their start and end apart: 5, of which 1 were waited for; matrix products, arithmetic and copies ran while one was open for 21% of the time, Pallas kernels for 0%

commit v1 on v0

--- a/solution.py
+++ b/solution.py
@@ -82,7 +82,12 @@
     value_summary = compress(jnp.concatenate([values, next_values], 0), pool_v, groups)
     place = start + jnp.arange(length)
     query_group = queries.reshape(length, groups, per_group, DH).transpose(1, 2, 0, 3)
-    part_keys = lax.all_gather(key_summary, "kv", axis=0, tiled=True)
+    ring = [key_summary]
+    for hop in range(3):
+        ring.append(lax.ppermute(ring[-1], "kv", [(dev, (dev + 1) % 4) for dev in range(4)]))
+    part_keys = jnp.roll(
+        jnp.concatenate(ring[::-1], axis=0), (lax.axis_index("kv") + 1) * ring[0].shape[0], axis=0
+    )
     part_values = lax.all_gather(value_summary, "kv", axis=0, tiled=True)
     count = part_keys.shape[0]
     ends = jnp.arange(count) * CMP_STRIDE + CMP_BLOCK - 1

time: 115 us -> 115 us (level)
  blocking collectives: 27 us -> 13.1 us
  waiting for transfers between devices: 1.22 us -> 9.87 us
  starting transfers between devices: 21 us -> 23.9 us
  local copies, waits for them, and re-layouts: 29.9 us -> 31.6 us
    all_gather x1 -> x0, blocking collectives: 13.3 us -> none  [per_device(): part_keys = lax.all_gather(key_summary, 'kv', axis=0, tiled=True)]
    ppermute x0 -> x3, waiting for transfers between devices: none -> 8.65 us  [per_device(): lax.ppermute(ring[-1], 'kv', [(dev, (dev + 1) % 4) for dev in range(4)])]
    ppermute x0 -> x3, starting transfers between devices: none -> 2.29 us  [per_device(): lax.ppermute(ring[-1], 'kv', [(dev, (dev + 1) % 4) for dev in range(4)])]
    mul x2, local copies, waits for them, and re-layouts: 1.7 us -> 3.3 us  [attend(): score = score.reshape(groups, per_group, QB, NSEL * SLC) * scale]
    unnamed x21 -> x28, local copies, waits for them, and re-layouts: 5.66 us -> 5.74 us
  transfers between devices with their start and end apart: 5 -> 8, of which waited for: 1 -> 3; matrix products, arithmetic and copies ran while one was open for 21% -> 21% of each run, Pallas kernels for 0% -> 0%
where the time goes in v1:
time: 115 us; the launch traced here: 114 us
  local copies, waits for them, and re-layouts  31.6 us (27%)
  starting transfers between devices  23.9 us (21%)
  other arithmetic  22.1 us (19%)
  blocking collectives  13.1 us (11%)
  matrix products  11.1 us (10%)
  waiting for transfers between devices  9.87 us (9%)
  loops' own time  1.71 us (1%)
    all_gather x1, blocking collectives, per_device(): part_values = lax.all_gather(value_summary, 'kv', axis=0, tiled=True)  13.1 us
    ppermute x3, waiting for transfers between devices, per_device(): lax.ppermute(ring[-1], 'kv', [(dev, (dev + 1) % 4) for dev in range(4)])  8.65 us
    all_to_all x1, starting transfers between devices, per_device(): lax.all_to_all(served[1], 'kv', split_axis=0, concat_axis=0, tiled=True)  7.44 us
    all_to_all x1, starting transfers between devices, per_device(): lax.all_to_all(asked_ids, 'kv', split_axis=0, concat_axis=0, tiled=True)  6.35 us
    unnamed x28, local copies, waits for them, and re-layouts  5.74 us
    all_to_all x1, starting transfers between devices, per_device(): lax.all_to_all(served[0], 'kv', split_axis=0, concat_axis=0, tiled=True)  5.29 us
    dot_general x2, matrix products, attend(): jnp.einsum('tghd,gnkd->ghtnk', query_part, keys_part, preferred_element_t...  5.03 us
    convert_element_type x2, other arithmetic, attend(): weight.astype(jnp.bfloat16)  4.81 us
  transfers between devices with their start and end apart: 8, of which 3 were waited for; matrix products, arithmetic and copies ran while one was open for 21% of the time, Pallas kernels for 0%

profile of v1, /device:TPU:0, one launch (start us, length us, event | category | flops | bytes accessed | tf_op | source)
XLA Modules:
  0.0 114.0 jit_solution(4192023715463981987)
XLA Ops:
  2.6 6.3 %all-to-all-start = ((s32[4,4,2]{1,2,0:T(2,128)}), s32[4,4,2]{1,2,0:T(2,128)S(1)}, u32[]{:S(2)}, u32[]{:S(2)}) async-start(s32[4,4,2]{1,2,0:T(2,128)} %copy.74), calls=%async_computation | async-start | bytes 8192 | tf_op jit(solution)/shard_map/all_to_all | solution.py:134
  9.6 1.3 %collective-permute-start.4 = (bf16[16,256]{1,0:T(8,128)(2,1)S(1)}, bf16[16,256]{1,0:T(8,128)(2,1)S(1)}, u32[]{:S(2)}, u32[]{:S(2)}) collective-permute-start(bf16[16,256]{1,0:T(8,128)(2,1)S(1)} %slice_bitcast_fusion.1), channel_id=1, source_target_pairs={{2,0},{4,2},{6,4},{3,1},{5,3},{7,5},{10,8},{12,10},{14,12},{11,9},... | collective-permute-start | bytes 24584 | tf_op jit(solution)/shard_map/ppermute | solution.py:21
  11.6 1.3 %collective-permute-start = (bf16[16,256]{1,0:T(8,128)(2,1)S(1)}, bf16[16,256]{1,0:T(8,128)(2,1)S(1)}, u32[]{:S(2)}, u32[]{:S(2)}) collective-permute-start(bf16[16,256]{1,0:T(8,128)(2,1)S(1)} %slice_bitcast_fusion.4), channel_id=1, source_target_pairs={{2,0},{4,2},{6,4},{3,1},{5,3},{7,5},{10,8},{12,10},{14,12},{11,9},... | collective-permute-start | bytes 24584 | tf_op jit(solution)/shard_map/ppermute | solution.py:21
  14.8 1.1 reshape_squeeze.9
  15.8 1.1 slice.65
  16.9 1.1 slice.72
  18.1 1.5 %gather_fusion.1 = s32[128]{0:T(128)S(1)} fusion(s32[4,16]{1,0:T(4,128)S(1)} %convert_subtract_fusion, s32[128]{0:T(128)S(1)} %reshape.454), kind=kCustom, calls=%fused_computation.1 | custom fusion | bytes 2048 | tf_op jit(solution)/shard_map/gather | solution.py:149
  26.7 1.1 reshape.513
  27.8 7.4 %all-to-all-start.2 = ((bf16[4,2,16384]{2,1,0:T(2,128)(2,1)}), bf16[4,2,16384]{2,1,0:T(2,128)(2,1)S(1)}, u32[]{:S(2)}, u32[]{:S(2)}) async-start(bf16[4,2,16384]{2,1,0:T(2,128)(2,1)} %reshape.513), calls=%async_computation.2 | async-start | bytes 524288 | tf_op jit(solution)/shard_map/all_to_all | solution.py:140
  36.0 1.1 reshape.511
  37.7 2.1 %collective-permute-start.1 = (bf16[16,4,64]{2,0,1:T(8,128)(2,1)S(1)}, bf16[16,4,64]{2,0,1:T(8,128)(2,1)S(1)}, u32[]{:S(2)}, u32[]{:S(2)}) collective-permute-start(bf16[16,4,64]{2,0,1:T(8,128)(2,1)S(1)} %fusion.40), channel_id=1, source_target_pairs={{0,2},{2,4},{4,6},{6,0},{1,3},{3,5},{5,7},{7,1},{8,10},{10,12},{12... | collective-permute-start | bytes 24584 | tf_op jit(solution)/shard_map/ppermute | solution.py:87
  39.9 3.3 %collective-permute-done.1 = bf16[16,4,64]{2,0,1:T(8,128)(2,1)S(1)} collective-permute-done((bf16[16,4,64]{2,0,1:T(8,128)(2,1)S(1)}, bf16[16,4,64]{2,0,1:T(8,128)(2,1)S(1)}, u32[]{:S(2)}, u32[]{:S(2)}) %collective-permute-start.1) | collective-permute-done | bytes 8224 | tf_op jit(solution)/shard_map/ppermute | solution.py:87
  43.5 5.3 %collective-permute-done.2 = bf16[16,4,64]{2,0,1:T(8,128)(2,1)S(1)} collective-permute-done((bf16[16,4,64]{2,0,1:T(8,128)(2,1)S(1)}, bf16[16,4,64]{2,0,1:T(8,128)(2,1)S(1)}, u32[]{:S(2)}, u32[]{:S(2)}) %collective-permute-start.2) | collective-permute-done | bytes 8224 | tf_op jit(solution)/shard_map/ppermute | solution.py:87
  48.8 13.1 %all_gather.3 = bf16[64,4,64]{2,1,0:T(4,128)(2,1)S(1)} all-gather(bf16[16,4,64]{2,1,0:T(4,128)(2,1)S(1)} %fusion.39), channel_id=1, replica_groups=mesh['grp'=2,'dp'=2,'kv'=4,'tp'=2] {'kv'}, dimensions={0}, use_global_device_ids=true | all-gather | bytes 40960 | tf_op jit(solution)/shard_map/all_gather | solution.py:91
  62.2 5.3 %all-to-all-start.1 = ((bf16[4,2,16384]{2,1,0:T(2,128)(2,1)}), bf16[4,2,16384]{2,1,0:T(2,128)(2,1)S(1)}, u32[]{:S(2)}, u32[]{:S(2)}) async-start(bf16[4,2,16384]{2,1,0:T(2,128)(2,1)} %reshape.511), calls=%async_computation.1 | async-start | bytes 524288 | tf_op jit(solution)/shard_map/all_to_all | solution.py:139
  67.5 5.2 %while.24 = (s32[]{:T(128)}, f32[4,4,256]{2,1,0:T(4,128)S(1)}, f32[4,4,256,64]{2,3,1,0:T(8,128)}, bf16[4,4,256,64]{2,3,1,0:T(8,128)(2,1)S(1)}, bf16[4,64,64]{2,1...) while((s32[]{:T(128)}, f32[4,4,256]{2,1,0:T(4,128)S(1)}, ...), condition=%wide.region_3.4_spmd.clone, body=%wide.region_0.3_spmd.clone.sunk | while | flops 17454080 | bytes 1326441 | solution.py:118
  73.0 1.2 %all-to-all-done.1 = bf16[4,2,16384]{2,1,0:T(2,128)(2,1)S(1)} async-done(((bf16[4,2,16384]{2,1,0:T(2,128)(2,1)}), bf16[4,2,16384]{2,1,0:T(2,128)(2,1)S(1)}, u32[]{:S(2)}, u32[]{:S(2)}) %all-to-all-start.1) | async-done | bytes 262176 | tf_op jit(solution)/shard_map/all_to_all | solution.py:139
  75.0 2.3 %gather_fusion.2 = bf16[128,64,64]{2,1,0:T(8,128)(2,1)} fusion(bf16[4,12,64,64]{3,2,1,0:T(8,128)(2,1)S(1)} %pad_maximum_fusion, s32[128]{0:T(128)S(1)} %reshape.460), kind=kCustom, calls=%fused_computation.2 | custom fusion | bytes 2098176 | tf_op jit(solution)/shard_map/gather | solution.py:150
  77.3 1.1 gather_fusion.4
  78.4 29.8 %while.23 = (s32[]{:T(128)}, f32[2,4,4,128,64]{3,4,2,1,0:T(8,128)}, s32[2,4,16]{2,1,0:T(4,128)S(1)}, s32[2]{0:T(128)S(1)}, s32[]{:T(128)}, /*index=5*/bf16[2,4,1...) while((s32[]{:T(128)}, f32[2,4,4,128,64]{3,4,2,1,0:T(8,128)}, ...), condition=%wide.region_10.11_spmd, body=%wide.region_7.10_spmd.sunk | while | flops 562172224 | bytes 65482908 | solution.py:180
  81.3 1.4 %compare_and_fusion.5 = pred[4,128,1024]{1,2,0:T(8,128)(4,1)S(1)} fusion(s32[128]{0:T(128)S(1)} %iota_add_fusion.5, s32[4,1024]{1,0:T(4,128)S(1)} %broadcast_add_fusion.2, pred[4,1024]{1,0:T(4,128)(4,1)S(1)} %and.117), kind=kLoop, calls=%fused_computation.15.clone.1 | loop fusion | flops 1048576 | bytes 545280 | tf_op jit(solution)/shard_map/while/body/eval_jaxpr/and | solution.py:166
  82.7 2.5 %select_reduce_fusion.5 = (f32[4,4,128]{2,1,0:T(4,128)S(1)}, f32[4,4,128,16,64]{2,4,1,3,0:T(8,128)S(1)}) fusion(pred[4,128,16,64]{1,3,2,0:T(8,128)(4,1)S(1)} %compare_and_fusion.4, bf16[2,128,4,4,64]{1,4,3,2,0:T(8,128)(2,1)} %get-tuple-element.346, s32[]{:T(128)S(6)} %copy.143, bf16[2,4,16,64,64]{4,3,2,1,0:T(8,128)(2,1)} %get-tuple-element.345), kind=kOutput, calls=%fused_computation.13.clone.1 | convolution fusion | flops 274724864 | bytes 10232832 | tf_op jit(solution)/shard_map/while/body/eval_jaxpr/tghd,gnkd->ghtnk/dot_general | solution.py:157
  85.3 2.1 %select_reduce_fusion.6 = f32[4,4,128]{2,1,0:T(4,128)S(1)} fusion(f32[4,4,128,16,64]{2,4,1,3,0:T(8,128)S(1)} %get-tuple-element.306, f32[4,4,128]{2,1,0:T(4,128)S(1)} %get-tuple-element.307, pred[4,128,16,64]{1,3,2,0:T(8,128)(4,1)S(1)} %compare_and_fusion.4), kind=kLoop, calls=%fused_computation.11.clone.1 | loop fusion | flops 8386560 | bytes 8929280 | tf_op jit(solution)/shard_map/while/body/eval_jaxpr/reduce_sum | solution.py:170
  87.4 1.7 %copy.137 = f32[4,4,128,16,64]{2,4,3,1,0:T(8,128)S(1)} copy(f32[4,4,128,16,64]{2,4,1,3,0:T(8,128)S(1)} %get-tuple-element.306) | data formatting | bytes 16777216 | tf_op jit(solution)/shard_map/while/body/eval_jaxpr/mul | solution.py:160
  89.1 2.4 %fusion.68 = bf16[4,4,128,1024]{2,3,1,0:T(8,128)(2,1)S(1)} fusion(f32[4,4,128,16,64]{2,4,3,1,0:T(8,128)S(1)} %copy.137, f32[4,4,128]{2,1,0:T(4,128)S(1)} %get-tuple-element.307, pred[4,128,1024]{1,2,0:T(8,128)(4,1)S(1)} %compare_and_fusion.5), kind=kLoop, calls=%fused_computation.10.clone.1 | loop fusion | flops 8388608 | bytes 13115392 | tf_op jit(solution)/shard_map/while/body/eval_jaxpr/convert_element_type | solution.py:174
  96.2 1.4 %compare_and_fusion.5 = pred[4,128,1024]{1,2,0:T(8,128)(4,1)S(1)} fusion(s32[128]{0:T(128)S(1)} %iota_add_fusion.5, s32[4,1024]{1,0:T(4,128)S(1)} %broadcast_add_fusion.2, pred[4,1024]{1,0:T(4,128)(4,1)S(1)} %and.117), kind=kLoop, calls=%fused_computation.15.clone.1 | loop fusion | flops 1048576 | bytes 545280 | tf_op jit(solution)/shard_map/while/body/eval_jaxpr/and | solution.py:166
  97.7 2.5 %select_reduce_fusion.5 = (f32[4,4,128]{2,1,0:T(4,128)S(1)}, f32[4,4,128,16,64]{2,4,1,3,0:T(8,128)S(1)}) fusion(pred[4,128,16,64]{1,3,2,0:T(8,128)(4,1)S(1)} %compare_and_fusion.4, bf16[2,128,4,4,64]{1,4,3,2,0:T(8,128)(2,1)} %get-tuple-element.346, s32[]{:T(128)S(6)} %copy.143, bf16[2,4,16,64,64]{4,3,2,1,0:T(8,128)(2,1)} %get-tuple-element.345), kind=kOutput, calls=%fused_computation.13.clone.1 | convolution fusion | flops 274724864 | bytes 10232832 | tf_op jit(solution)/shard_map/while/body/eval_jaxpr/tghd,gnkd->ghtnk/dot_general | solution.py:157
  100.2 2.1 %select_reduce_fusion.6 = f32[4,4,128]{2,1,0:T(4,128)S(1)} fusion(f32[4,4,128,16,64]{2,4,1,3,0:T(8,128)S(1)} %get-tuple-element.306, f32[4,4,128]{2,1,0:T(4,128)S(1)} %get-tuple-element.307, pred[4,128,16,64]{1,3,2,0:T(8,128)(4,1)S(1)} %compare_and_fusion.4), kind=kLoop, calls=%fused_computation.11.clone.1 | loop fusion | flops 8386560 | bytes 8929280 | tf_op jit(solution)/shard_map/while/body/eval_jaxpr/reduce_sum | solution.py:170
  102.3 1.7 %copy.137 = f32[4,4,128,16,64]{2,4,3,1,0:T(8,128)S(1)} copy(f32[4,4,128,16,64]{2,4,1,3,0:T(8,128)S(1)} %get-tuple-element.306) | data formatting | bytes 16777216 | tf_op jit(solution)/shard_map/while/body/eval_jaxpr/mul | solution.py:160
  104.0 2.4 %fusion.68 = bf16[4,4,128,1024]{2,3,1,0:T(8,128)(2,1)S(1)} fusion(f32[4,4,128,16,64]{2,4,3,1,0:T(8,128)S(1)} %copy.137, f32[4,4,128]{2,1,0:T(4,128)S(1)} %get-tuple-element.307, pred[4,128,1024]{1,2,0:T(8,128)(4,1)S(1)} %compare_and_fusion.5), kind=kLoop, calls=%fused_computation.10.clone.1 | loop fusion | flops 8388608 | bytes 13115392 | tf_op jit(solution)/shard_map/while/body/eval_jaxpr/convert_element_type | solution.py:174
  108.2 1.6 %fusion.33 = (f32[256,4,4]{0,2,1:T(4,128)S(1)}, f32[4,4,256,64]{2,3,1,0:T(8,128)S(1)}) fusion(f32[256,4,4]{0,2,1:T(4,128)S(1)} %mul.294, f32[256,4,4]{0,2,1:T(4,128)S(1)} %mul.291, f32[4,4,256,64]{2,3,1,0:T(8,128)S(1)} %copy-done.4, f32[4,4,256]{2,1,0:T(4,128)S(1)} %broadcast_maximum_fusion.1, f32[2,4,4,128,64]{3,4,2,1,0:T(8,128)} %get-tuple-element.87), kind=kLoop, calls=%fused_computation.57 | loop fusion | flops 1568768 | bytes 3211264 | tf_op jit(solution)/shard_map/reduce_sum | solution.py:187
  109.9 2.0 %copy.86 = f32[2,128,4,4,64]{1,0,4,3,2:T(2,128)S(1)} copy(f32[2,128,4,4,64]{1,4,3,2,0:T(8,128)} %bitcast.234) | data formatting | bytes 2097152 | tf_op jit(solution)/shard_map/transpose | solution.py:183
  (166 shorter events, 30.9 us)
Async XLA Ops:
  0.0 23.9 %copy-start.5 = (bf16[1,256,1024]{2,1,0:T(8,128)(2,1)S(1)}, bf16[1,256,1024]{2,1,0:T(8,128)(2,1)}, u32[]{:S(2)}) copy-start(bf16[1,256,1024]{2,1,0:T(8,128)(2,1)} %param.12) | copy-start | bytes 1572868
  2.6 23.2 %all-to-all-start = ((s32[4,4,2]{1,2,0:T(2,128)}), s32[4,4,2]{1,2,0:T(2,128)S(1)}, u32[]{:S(2)}, u32[]{:S(2)}) async-start(s32[4,4,2]{1,2,0:T(2,128)} %copy.74), calls=%async_computation | async-start | bytes 8192 | tf_op jit(solution)/shard_map/all_to_all | solution.py:134
  9.6 27.4 %collective-permute-start.4 = (bf16[16,256]{1,0:T(8,128)(2,1)S(1)}, bf16[16,256]{1,0:T(8,128)(2,1)S(1)}, u32[]{:S(2)}, u32[]{:S(2)}) collective-permute-start(bf16[16,256]{1,0:T(8,128)(2,1)S(1)} %slice_bitcast_fusion.1), channel_id=1, source_target_pairs={{2,0},{4,2},{6,4},{3,1},{5,3},{7,5},{10,8},{12,10},{14,12},{11,9},... | collective-permute-start | bytes 24584 | tf_op jit(solution)/shard_map/ppermute | solution.py:21
  11.6 25.6 %collective-permute-start = (bf16[16,256]{1,0:T(8,128)(2,1)S(1)}, bf16[16,256]{1,0:T(8,128)(2,1)S(1)}, u32[]{:S(2)}, u32[]{:S(2)}) collective-permute-start(bf16[16,256]{1,0:T(8,128)(2,1)S(1)} %slice_bitcast_fusion.4), channel_id=1, source_target_pairs={{2,0},{4,2},{6,4},{3,1},{5,3},{7,5},{10,8},{12,10},{14,12},{11,9},... | collective-permute-start | bytes 24584 | tf_op jit(solution)/shard_map/ppermute | solution.py:21
  19.7 17.4 %copy-start.2 = (bf16[1,256,256]{2,1,0:T(8,128)(2,1)S(1)}, bf16[1,256,256]{2,1,0:T(8,128)(2,1)}, u32[]{:S(2)}) copy-start(bf16[1,256,256]{2,1,0:T(8,128)(2,1)} %param.14) | copy-start | bytes 393220
  22.8 14.5 %copy-start.3 = (bf16[1,256,256]{2,1,0:T(8,128)(2,1)S(1)}, bf16[1,256,256]{2,1,0:T(8,128)(2,1)}, u32[]{:S(2)}) copy-start(bf16[1,256,256]{2,1,0:T(8,128)(2,1)} %param.13) | copy-start | bytes 393220
  27.8 34.3 %all-to-all-start.2 = ((bf16[4,2,16384]{2,1,0:T(2,128)(2,1)}), bf16[4,2,16384]{2,1,0:T(2,128)(2,1)S(1)}, u32[]{:S(2)}, u32[]{:S(2)}) async-start(bf16[4,2,16384]{2,1,0:T(2,128)(2,1)} %reshape.513), calls=%async_computation.2 | async-start | bytes 524288 | tf_op jit(solution)/shard_map/all_to_all | solution.py:140
  37.7 5.6 %collective-permute-start.1 = (bf16[16,4,64]{2,0,1:T(8,128)(2,1)S(1)}, bf16[16,4,64]{2,0,1:T(8,128)(2,1)S(1)}, u32[]{:S(2)}, u32[]{:S(2)}) collective-permute-start(bf16[16,4,64]{2,0,1:T(8,128)(2,1)S(1)} %fusion.40), channel_id=1, source_target_pairs={{0,2},{2,4},{4,6},{6,0},{1,3},{3,5},{5,7},{7,1},{8,10},{10,12},{12... | collective-permute-start | bytes 24584 | tf_op jit(solution)/shard_map/ppermute | solution.py:87
  43.3 5.5 %collective-permute-start.2 = (bf16[16,4,64]{2,0,1:T(8,128)(2,1)S(1)}, bf16[16,4,64]{2,0,1:T(8,128)(2,1)S(1)}, u32[]{:S(2)}, u32[]{:S(2)}) collective-permute-start(bf16[16,4,64]{2,0,1:T(8,128)(2,1)S(1)} %collective-permute-done.1), channel_id=1, source_target_pairs={{0,2},{2,4},{4,6},{6,0},{1,3},{3,5},{5,7},{7,1},{8,10},{10,12},{12... | collective-permute-start | bytes 24584 | tf_op jit(solution)/shard_map/ppermute | solution.py:87
  48.8 13.2 %collective-permute-start.3 = (bf16[16,4,64]{2,0,1:T(8,128)(2,1)S(1)}, bf16[16,4,64]{2,0,1:T(8,128)(2,1)S(1)}, u32[]{:S(2)}, u32[]{:S(2)}) collective-permute-start(bf16[16,4,64]{2,0,1:T(8,128)(2,1)S(1)} %collective-permute-done.2), channel_id=1, source_target_pairs={{0,2},{2,4},{4,6},{6,0},{1,3},{3,5},{5,7},{7,1},{8,10},{10,12},{12... | collective-permute-start | bytes 24584 | tf_op jit(solution)/shard_map/ppermute | solution.py:87
  62.2 12.1 %all-to-all-start.1 = ((bf16[4,2,16384]{2,1,0:T(2,128)(2,1)}), bf16[4,2,16384]{2,1,0:T(2,128)(2,1)S(1)}, u32[]{:S(2)}, u32[]{:S(2)}) async-start(bf16[4,2,16384]{2,1,0:T(2,128)(2,1)} %reshape.511), calls=%async_computation.1 | async-start | bytes 524288 | tf_op jit(solution)/shard_map/all_to_all | solution.py:139
  72.6 5.7 %copy-start.6 = (s32[1,2,4,16]{3,2,1,0:T(4,128)S(1)}, s32[1,2,4,16]{3,2,1,0:T(4,128)}, u32[]{:S(2)}) copy-start(s32[1,2,4,16]{3,2,1,0:T(4,128)} %param.16) | copy-start | bytes 1540
  78.4 29.9 %copy-start.4 = (f32[4,4,256,64]{2,3,1,0:T(8,128)S(1)}, f32[4,4,256,64]{2,3,1,0:T(8,128)}, u32[]{:S(2)}) copy-start(f32[4,4,256,64]{2,3,1,0:T(8,128)} %get-tuple-element.85) | copy-start | bytes 3145732
  78.4 34.4 %copy-start.7 = (f32[1024]{0:T(1024)S(1)}, f32[1024]{0:T(1024)}, u32[]{:S(2)}) copy-start(f32[1024]{0:T(1024)} %param.19) | copy-start | bytes 12292
  89.0 2.4 %copy-start = (f32[2,4,4,128,64]{3,4,2,1,0:T(8,128)S(1)}, f32[2,4,4,128,64]{3,4,2,1,0:T(8,128)}, u32[]{:S(2)}) copy-start(f32[2,4,4,128,64]{3,4,2,1,0:T(8,128)} %get-tuple-element.331) | copy-start | bytes 3145732 | tf_op jit(solution)/shard_map/while
  92.3 1.0 copy-start.1
  104.0 2.4 %copy-start = (f32[2,4,4,128,64]{3,4,2,1,0:T(8,128)S(1)}, f32[2,4,4,128,64]{3,4,2,1,0:T(8,128)}, u32[]{:S(2)}) copy-start(f32[2,4,4,128,64]{3,4,2,1,0:T(8,128)} %get-tuple-element.331) | copy-start | bytes 3145732 | tf_op jit(solution)/shard_map/while
  107.3 1.0 copy-start.1
